TPU v7x, 32 devices: a whole 2x2x4 slice. The times are simulated.
32 devices in a mesh: ep: 8 (over z, x), tp: 4 (over y, core).
Axes of the slice: x: 2, y: 2, z: 4, core: 2. Of those that a mesh axis runs over, the one named last changes fastest.
Arguments:
- query_rows: bfloat16 [4096, 3072], P('ep', 'tp'), may hold values from -6 to 6
- key_rows: bfloat16 [4096, 1024], P('ep', 'tp'), may hold values from -6 to 6
- value_rows: bfloat16 [4096, 1024], P('ep', 'tp'), may hold values from -6 to 6
- query_gain: float32 [48, 64], P('tp'), may hold values from 0.4 to 48
- key_gain: float32 [16, 64], P('tp'), may hold values from 0.1 to 1.9
- sink_logits: float32 [48], P('tp'), may hold values from 1 to 6
- out_weight: bfloat16 [3072, 2048], P('tp'), may hold values from -0.109375 to 0.109375
- expert_input: bfloat16 [4096, 2048], P(('ep', 'tp')), may hold values from -6 to 6
- expert_gain: float32 [2048], replicated, may hold values from 0.1 to 1.9
- routes: int32 [4096, 2], P(('ep', 'tp')), may hold values from 0 to 31, all different within a row; in each aligned block of 128 rows (0 to 127, 128 to 255, ...) at most 12 rows name the same one
- route_logits: float32 [4096, 2], P(('ep', 'tp')), may hold values from -6 to 6
- gate_weight: bfloat16 [32, 2048, 2048], P('ep', None, 'tp'), may hold values from -0.375 to 0.375
- up_weight: bfloat16 [32, 2048, 2048], P('ep', None, 'tp'), may hold values from -0.375 to 0.375
- down_weight: bfloat16 [32, 2048, 2048], P('ep', 'tp'), may hold values from -0.01953125 to 0.01953125
Outputs:
- attended: bfloat16 [4096, 2048], P(('ep', 'tp'))
- expert_mix: bfloat16 [4096, 2048], P(('ep', 'tp'))
Inputs may be any that keep to these rules, and one draw needn't show every extreme that they name: `routes`: each row names 2 different experts; in the rows of one device no expert is named more than 12 times, and in some device one expert is named exactly 12 times.
All inputs are finite; a program needn't handle non-finite values.
Results may differ from a plain program's by a relative error of at most 0.017.
The roundings to bfloat16 on the way count: a program that leaves them out, or rounds other values in their place, can miss the bound.
Values may be sent and summed in bfloat16 or wider, within the bound.
A program may use at most 128 MiB of HBM per device.

v0:
```python
import jax
import jax.numpy as jnp
from jax import lax
from jax.sharding import PartitionSpec as P

EXPERTS = 32
WINDOW = 128


EPSILON = 1e-06
CLAMP_LIMIT = 7.0
ACT_SLOPE = 1.702
NEGATIVE = -1e30


def shifted(value, axis, steps):
    count = lax.axis_size(axis)
    initial, last = (max(0, -steps), min(count, count - steps))
    return lax.ppermute(value, axis, [(source, source + steps) for source in range(initial, last)])


def head_norm(row_data, gain_table):
    head_count, head_size = gain_table.shape
    widened = row_data.astype(jnp.float32).reshape(row_data.shape[0], head_count, head_size)
    scaled = widened * lax.rsqrt(jnp.mean(widened * widened, axis=-1, keepdims=True) + EPSILON)
    return (scaled * gain_table).astype(jnp.bfloat16)


def band(padded, blocks):
    tiled = padded.reshape((blocks + 1, WINDOW) + padded.shape[1:])
    return jnp.concatenate([tiled[:-1], tiled[1:]], axis=1)


def attend(query_rows, key_rows, value_rows, query_gain, key_gain, sink_logits):
    seq_rows = query_rows.shape[0]
    key_heads, head_size = key_gain.shape
    group_size = query_gain.shape[0] // key_heads
    blocks = seq_rows // WINDOW
    query_hat = head_norm(query_rows, query_gain).reshape(
        blocks, WINDOW, key_heads, group_size, head_size
    )
    key_hat = head_norm(key_rows, key_gain)
    value_hat = value_rows.reshape(seq_rows, key_heads, head_size)
    tail_rows = jnp.stack([key_hat[seq_rows - WINDOW :], value_hat[seq_rows - WINDOW :]])
    earlier = shifted(tail_rows, "ep", 1)
    key_band = band(jnp.concatenate([earlier[0], key_hat], axis=0), blocks)
    value_band = band(jnp.concatenate([earlier[1], value_hat], axis=0), blocks)
    query_pos = lax.broadcasted_iota(jnp.int32, (WINDOW, 2 * WINDOW), 0)
    key_pos = lax.broadcasted_iota(jnp.int32, (WINDOW, 2 * WINDOW), 1)
    distance = query_pos + WINDOW - key_pos
    inside = (distance >= 0) & (distance < WINDOW)
    first_block = (lax.broadcasted_iota(jnp.int32, (blocks, 1, 1), 0) == 0) & (
        lax.axis_index("ep") == 0
    )
    allowed = inside[None] & ~(first_block & (key_pos < WINDOW)[None])
    scores = jnp.einsum(
        "bqkgd,bjkd->bkgqj", query_hat, key_band, preferred_element_type=jnp.float32
    ) * head_size ** (-0.5)
    scores = jnp.where(allowed[:, None, None], scores, NEGATIVE)
    sink_table = sink_logits.reshape(1, key_heads, group_size, 1, 1)
    highest = jnp.maximum(jnp.max(scores, axis=-1, keepdims=True), sink_table)
    weights = jnp.exp(scores - highest)
    total = jnp.sum(weights, axis=-1, keepdims=True) + jnp.exp(sink_table - highest)
    mixed = jnp.einsum(
        "bkgqj,bjkd->bkgqd",
        weights.astype(jnp.bfloat16),
        value_band,
        preferred_element_type=jnp.float32,
    )
    mixed = (mixed / total).astype(jnp.bfloat16)
    return jnp.transpose(mixed, (0, 3, 1, 2, 4)).reshape(seq_rows, -1)


def slot_maps(route_block, capacity):
    flat_routes = route_block.reshape(-1)
    expert_hot = (flat_routes[:, None] == lax.broadcasted_iota(jnp.int32, (1, EXPERTS), 1)).astype(
        jnp.int32
    )
    before = jnp.cumsum(expert_hot, axis=0) - expert_hot
    position = jnp.sum(before * expert_hot, axis=1)
    place_hot = (position[:, None] == lax.broadcasted_iota(jnp.int32, (1, capacity), 1)).astype(
        jnp.float32
    )
    row_total, fanout = route_block.shape
    return (
        expert_hot.astype(jnp.float32).reshape(row_total, fanout, EXPERTS),
        place_hot.reshape(row_total, fanout, capacity),
    )


def dispatch_matrix(route_block, capacity):
    expert_hot, place_hot = slot_maps(route_block, capacity)
    return jnp.einsum("rke,rkc->ecr", expert_hot, place_hot).astype(jnp.bfloat16)


def combine_matrix(route_block, route_weight, capacity):
    expert_hot, place_hot = slot_maps(route_block, capacity)
    return jnp.einsum(
        "rke,rkc,rk->rec", expert_hot, place_hot, route_weight, precision=lax.Precision.HIGHEST
    )


def expert_hidden(piece, gate_weight, up_weight):
    gate_pre = jnp.einsum("aecd,edf->aecf", piece, gate_weight, preferred_element_type=jnp.float32)
    up_pre = jnp.einsum("aecd,edf->aecf", piece, up_weight, preferred_element_type=jnp.float32)
    clipped = jnp.minimum(gate_pre, CLAMP_LIMIT)
    linear = jnp.clip(up_pre, -CLAMP_LIMIT, CLAMP_LIMIT)
    return (clipped * jax.nn.sigmoid(ACT_SLOPE * clipped) * (linear + 1.0)).astype(jnp.bfloat16)


def on_device(
    query_rows,
    key_rows,
    value_rows,
    query_gain,
    key_gain,
    sink_logits,
    out_weight,
    expert_input,
    expert_gain,
    routes,
    route_logits,
    gate_weight,
    up_weight,
    down_weight,
):
    heads_out = attend(query_rows, key_rows, value_rows, query_gain, key_gain, sink_logits)
    attended = lax.psum_scatter(
        jnp.dot(heads_out, out_weight, preferred_element_type=jnp.float32).astype(jnp.bfloat16),
        "tp",
        scatter_dimension=0,
        tiled=True,
    )
    own_rows = expert_input.shape[0]
    fanout = routes.shape[1]
    capacity = (3 * own_rows * fanout + 2 * EXPERTS - 1) // (2 * EXPERTS)
    ep_size = lax.axis_size("ep")
    tp_size = lax.axis_size("tp")
    local_experts = gate_weight.shape[0]
    widened = expert_input.astype(jnp.float32)
    normed = (
        widened
        * lax.rsqrt(jnp.mean(widened * widened, axis=-1, keepdims=True) + EPSILON)
        * expert_gain
    ).astype(jnp.bfloat16)
    route_weight = jax.nn.softmax(route_logits, axis=-1)
    combine = combine_matrix(routes, route_weight, capacity)
    sender = dispatch_matrix(routes, capacity)
    slot_rows = jnp.einsum(
        "ecr,rd->ecd", sender, normed, preferred_element_type=jnp.float32
    ).astype(jnp.bfloat16)
    slot_rows = slot_rows.reshape(ep_size, local_experts, capacity, -1)
    arrived = lax.all_to_all(slot_rows, "ep", split_axis=0, concat_axis=0, tiled=True)
    hidden_units = expert_hidden(
        lax.all_gather(arrived, "tp", axis=0, tiled=True), gate_weight, up_weight
    )
    partial_value = jnp.einsum(
        "aecf,efd->aecd", hidden_units, down_weight, preferred_element_type=jnp.float32
    ).astype(jnp.bfloat16)
    partial_value = partial_value.reshape(tp_size, ep_size * local_experts * capacity, -1)
    pieces = lax.all_to_all(partial_value, "tp", split_axis=0, concat_axis=0, tiled=True)
    summed = jnp.sum(pieces, axis=0, dtype=jnp.float32).astype(jnp.bfloat16)
    summed = summed.reshape(ep_size, local_experts * capacity, -1)
    returned = lax.all_to_all(summed, "ep", split_axis=0, concat_axis=0, tiled=True).reshape(
        EXPERTS, capacity, -1
    )
    expert_mix = jnp.einsum(
        "rec,ecd->rd", combine, returned.astype(jnp.float32), precision=lax.Precision.HIGHEST
    ).astype(jnp.bfloat16)
    return (attended, expert_mix)


def solution(mesh):
    placed = (
        P("ep", "tp"),
        P("ep", "tp"),
        P("ep", "tp"),
        P("tp", None),
        P("tp", None),
        P("tp"),
        P("tp", None),
        P(("ep", "tp"), None),
        P(),
        P(("ep", "tp"), None),
        P(("ep", "tp"), None),
        P("ep", None, "tp"),
        P("ep", None, "tp"),
        P("ep", "tp", None),
    )
    return jax.shard_map(
        on_device,
        mesh=mesh,
        in_specs=placed,
        out_specs=(P(("ep", "tp"), None), P(("ep", "tp"), None)),
        check_vma=False,
    )
```

profile of v0, /device:TPU:0, one launch (start us, length us, event | category | flops | bytes accessed | tf_op | source)
XLA Modules:
  0.0 307.8 jit_solution(13394188063534734135)
XLA Ops:
  7.2 0.9 copy.76
  8.5 0.6 reduce-window.6
  9.0 0.2 slice_reduce_fusion
  9.5 1.1 fusion.36
  10.6 1.2 fusion.37
  11.9 2.9 convolution_convert_fusion.1
  14.7 3.6 %reshape.180 = bf16[8,4,12,2048]{3,1,0,2:T(4,128)(2,1)} reshape(bf16[32,12,2048]{2,0,1:T(8,128)(2,1)} %convolution_convert_fusion.1) | data formatting | bytes 3145728 | tf_op jit(solution)/shard_map/reshape | solution.py:152
  18.4 2.1 copy.82
  20.5 44.1 %all_to_all.15 = bf16[8,4,12,2048]{3,1,2,0:T(4,128)(2,1)S(1)} all-to-all(bf16[8,4,12,2048]{3,1,2,0:T(4,128)(2,1)S(1)} %copy.82), channel_id=1, replica_groups=mesh['ep'=8,'tp'=4] {'ep'}, dimensions={0} | all-to-all | bytes 3145728 | tf_op jit(solution)/shard_map/all_to_all | solution.py:153
  64.6 2.0 copy.83
  66.6 1.1 copy.64
  67.7 1.8 copy.65
  69.5 0.8 slice.49
  70.6 0.7 copy-done.2
  71.3 0.7 pad_maximum_fusion.2
  72.0 4.0 %collective-permute-start = (bf16[2,128,4,64]{1,3,2,0:T(8,128)(2,1)}, bf16[2,128,4,64]{1,3,2,0:T(8,128)(2,1)}, u32[]{:S(2)}, u32[]{:S(2)}) collective-permute-start(bf16[2,128,4,64]{1,3,2,0:T(8,128)(2,1)} %pad_maximum_fusion.2), channel_id=1, source_target_pairs={{0,4},{4,8},{8,12},{12,16},{16,20},{20,24},{24,28},{1,5},{5,9},{9,... | collective-permute-start | bytes 393224 | tf_op jit(solution)/shard_map/ppermute | solution.py:19
  75.9 1.0 reshape.175
  76.9 2.0 reshape.191
  78.9 2.3 copy.68
  81.2 2.7 reshape.176
  83.9 2.6 convert_multiply_fusion.2
  86.5 1.6 reduce_sum.71
  88.3 2.0 copy.73
  90.3 0.5 iota_compare_fusion.5
  90.8 0.6 compare_and_fusion
  91.4 20.8 %all-gather.2.cloned.1.call-done = bf16[32,4,12,2048]{3,0,2,1:T(8,128)(2,1)} async-done(((bf16[8,4,12,2048]{3,0,2,1:T(8,128)(2,1)}), bf16[32,4,12,2048]{3,0,2,1:T(8,128)(2,1)}) %all-gather.2.cloned.1.call-update) | async-done | bytes 6291472 | tf_op jit(solution)/shard_map/all_gather | solution.py:155
  112.2 10.2 %fusion.2 = f32[4,32,12,512]{3,1,2,0:T(8,128)} fusion(bf16[32,4,12,2048]{3,0,2,1:T(8,128)(2,1)} %all-gather.2.cloned.1.call-done, bf16[4,2048,512]{2,1,0:T(8,128)(2,1)} %param.26), kind=kOutput, calls=%fused_computation.2 | convolution fusion | flops 3221225472 | bytes 17825792 | tf_op jit(solution)/shard_map/aecd,edf->aecf/dot_general | solution.py:105
  122.4 14.2 %convert_bitcast_fusion = bf16[32,4,12,2048]{3,0,2,1:T(8,128)(2,1)} fusion(bf16[4,512,2048]{2,1,0:T(8,128)(2,1)} %param.27, f32[4,32,12,512]{3,1,2,0:T(8,128)} %fusion.2, bf16[32,4,12,2048]{3,0,2,1:T(8,128)(2,1)} %all-gather.2.cloned.1.call-done, bf16[4,2048,512]{2,1,0:T(8,128)(2,1)} %param.25), kind=kOutput, calls=%fused_computation.7 | convolution fusion | flops 6453460992 | bytes 32505856 | tf_op jit(solution)/shard_map/aecf,efd->aecd/dot_general | solution.py:157
  136.6 9.7 %copy.84 = bf16[32,4,12,2048]{3,2,1,0:T(8,128)(2,1)} copy(bf16[32,4,12,2048]{3,0,2,1:T(8,128)(2,1)} %convert_bitcast_fusion) | data formatting | bytes 12582912 | tf_op jit(solution)/shard_map/convert_element_type | solution.py:159
  146.2 10.7 %reshape.181 = bf16[4,384,2048]{2,1,0:T(8,128)(2,1)} reshape(bf16[32,4,12,2048]{3,2,1,0:T(8,128)(2,1)} %copy.84) | data formatting | bytes 12582912 | tf_op jit(solution)/shard_map/reshape | solution.py:160
  156.9 5.2 %all-to-all-start.1 = ((bf16[4,384,2048]{2,1,0:T(8,128)(2,1)}), bf16[4,384,2048]{2,1,0:T(8,128)(2,1)}, u32[]{:S(2)}, u32[]{:S(2)}) async-start(bf16[4,384,2048]{2,1,0:T(8,128)(2,1)} %reshape.181), calls=%async_computation.2 | async-start | bytes 12582912 | tf_op jit(solution)/shard_map/all_to_all | solution.py:161
  162.2 0.3 reduce-scatter.2.cloned.1.call-start
  162.5 1.2 fusion.52
  163.7 2.1 multiply_convert_fusion
  165.8 0.2 not_and_fusion
  166.0 0.9 slice_bitcast_fusion.1
  167.1 1.1 fusion.8
  168.4 1.6 fusion.6
  170.1 1.6 fusion.27
  171.7 0.6 copy.75
  172.3 3.2 %convolution_convert_fusion = bf16[512,2048]{1,0:T(8,128)(2,1)} fusion(bf16[768,2048]{1,0:T(8,128)(2,1)S(1)} %copy-done, bf16[96,8,4,128]{3,2,1,0:T(4,128)(2,1)S(1)} %bitcast.148), kind=kOutput, calls=%fused_computation.25 | convolution fusion | flops 1611661312 | bytes 6029312 | tf_op jit(solution)/shard_map/dot_general | solution.py:129
  175.5 68.5 %all-to-all-done.1 = bf16[4,384,2048]{2,1,0:T(8,128)(2,1)} async-done(((bf16[4,384,2048]{2,1,0:T(8,128)(2,1)}), bf16[4,384,2048]{2,1,0:T(8,128)(2,1)}, u32[]{:S(2)}, u32[]{:S(2)}) %all-to-all-start.1) | async-done | bytes 6291488 | tf_op jit(solution)/shard_map/all_to_all | solution.py:161
  244.1 5.8 %reduce_sum.76 = bf16[384,2048]{1,0:T(8,128)(2,1)} reduce(bf16[4,384,2048]{2,1,0:T(8,128)(2,1)} %all-to-all-done.1, bf16[]{:T(256)} %constant.49.clone.1), dimensions={0}, to_apply=%region_11.12 | reduce | flops 2359296 | bytes 7864322 | tf_op jit(solution)/shard_map/reduce_sum | solution.py:162
  249.8 5.6 %all-to-all-start.2 = ((bf16[8,48,2048]{2,1,0:T(8,128)(2,1)}), bf16[8,48,2048]{2,1,0:T(8,128)(2,1)}, u32[]{:S(2)}, u32[]{:S(2)}) async-start(bf16[8,48,2048]{2,1,0:T(8,128)(2,1)} %bitcast.147), calls=%async_computation.3 | async-start | bytes 3145728 | tf_op jit(solution)/shard_map/all_to_all | solution.py:164
  255.7 3.2 %fusion.59 = f32[128,32,12]{1,2,0:T(8,128)} fusion(f32[128,2]{1,0:T(8,128)S(1)} %copy.80, s32[128,2]{1,0:T(8,128)S(1)} %copy-done.6, s32[128,2]{1,0:T(8,128)S(1)} %copy.76), kind=kOutput, calls=%fused_computation.76 | convolution fusion | flops 1210368 | bytes 199680 | tf_op jit(solution)/shard_map/rke,rkc,rk->rec/dot_general | solution.py:98
  258.9 33.4 %all-to-all-done.2 = bf16[8,48,2048]{2,1,0:T(8,128)(2,1)} async-done(((bf16[8,48,2048]{2,1,0:T(8,128)(2,1)}), bf16[8,48,2048]{2,1,0:T(8,128)(2,1)}, u32[]{:S(2)}, u32[]{:S(2)}) %all-to-all-start.2) | async-done | bytes 1572896 | tf_op jit(solution)/shard_map/all_to_all | solution.py:164
  292.3 3.6 %reshape.183 = bf16[32,12,2048]{2,1,0:T(8,128)(2,1)} reshape(bf16[8,48,2048]{2,1,0:T(8,128)(2,1)} %all-to-all-done.2) | data formatting | bytes 3145728 | tf_op jit(solution)/shard_map/reshape | solution.py:164
  295.9 5.1 %fusion.22 = bf16[128,2048]{1,0:T(8,128)(2,1)} fusion(bf16[32,12,2048]{2,1,0:T(8,128)(2,1)} %reshape.183, f32[128,32,12]{1,2,0:T(8,128)} %fusion.59), kind=kOutput, calls=%fused_computation.28 | convolution fusion | flops 1208221696 | bytes 2293760 | tf_op jit(solution)/shard_map/rec,ecd->rd/dot_general | solution.py:167
  (57 shorter events, 1.6 us)
Async XLA Ops:
  7.2 165.1 %copy-start = (bf16[768,2048]{1,0:T(8,128)(2,1)S(1)}, bf16[768,2048]{1,0:T(8,128)(2,1)}, u32[]{:S(2)}) copy-start(bf16[768,2048]{1,0:T(8,128)(2,1)} %param.20) | copy-start | bytes 9437188
  7.2 105.0 %all-gather.2.cloned.1.call-start = ((), (), s32[]{:S(2)}) async-start(), calls=%async_computation.5 | async-start | bytes 7864320 | tf_op jit(solution)/shard_map/all_gather | solution.py:155
  9.5 8.8 %copy-start.5 = (s32[128,2]{1,0:T(8,128)}, s32[128,2]{1,0:T(8,128)S(1)}, u32[]{:S(2)}) copy-start(s32[128,2]{1,0:T(8,128)S(1)} %eq.86) | copy-start | bytes 3076
  64.6 5.9 %copy-start.8 = (f32[4,64]{1,0:T(4,128)S(1)}, f32[4,64]{1,0:T(4,128)}, u32[]{:S(2)}) copy-start(f32[4,64]{1,0:T(4,128)} %param.18) | copy-start | bytes 3076
  70.6 0.7 copy-start.2
  72.0 94.0 %collective-permute-start = (bf16[2,128,4,64]{1,3,2,0:T(8,128)(2,1)}, bf16[2,128,4,64]{1,3,2,0:T(8,128)(2,1)}, u32[]{:S(2)}, u32[]{:S(2)}) collective-permute-start(bf16[2,128,4,64]{1,3,2,0:T(8,128)(2,1)} %pad_maximum_fusion.2), channel_id=1, source_target_pairs={{0,4},{4,8},{8,12},{12,16},{16,20},{20,24},{24,28},{1,5},{5,9},{9,... | collective-permute-start | bytes 393224 | tf_op jit(solution)/shard_map/ppermute | solution.py:19
  81.2 6.9 %copy-start.9 = (f32[12,64]{1,0:T(8,128)S(1)}, f32[12,64]{1,0:T(8,128)}, u32[]{:S(2)}) copy-start(f32[12,64]{1,0:T(8,128)} %param.17) | copy-start | bytes 9220
  81.2 7.0 %copy-start.12 = (f32[12]{0:T(128)S(1)}, f32[12]{0:T(128)}, u32[]{:S(2)}) copy-start(f32[12]{0:T(128)} %param.19) | copy-start | bytes 148
  156.9 87.2 %all-to-all-start.1 = ((bf16[4,384,2048]{2,1,0:T(8,128)(2,1)}), bf16[4,384,2048]{2,1,0:T(8,128)(2,1)}, u32[]{:S(2)}, u32[]{:S(2)}) async-start(bf16[4,384,2048]{2,1,0:T(8,128)(2,1)} %reshape.181), calls=%async_computation.2 | async-start | bytes 12582912 | tf_op jit(solution)/shard_map/all_to_all | solution.py:161
  162.2 4.7 %copy-start.1 = (bf16[512,256]{0,1:T(8,128)(2,1)S(1)}, bf16[512,256]{0,1:T(8,128)(2,1)}, u32[]{:S(2)}) copy-start(bf16[512,256]{0,1:T(8,128)(2,1)} %copy.65) | copy-start | bytes 786436
  162.2 138.8 %reduce-scatter.2.cloned.1.call-start = ((), (), s32[]{:S(2)}) async-start(), calls=%async_computation.4 | async-start | bytes 2621440 | tf_op jit(solution)/shard_map/reduce_scatter | solution.py:128
  162.5 3.4 %copy-start.10 = (pred[256]{0:T(512)(128)(4,1)S(1)}, pred[256]{0:T(512)(128)(4,1)}, u32[]{:S(2)}) copy-start(pred[256]{0:T(512)(128)(4,1)} %iota_compare_fusion.5) | copy-start | bytes 772
  162.5 3.4 %copy-start.11 = (pred[4]{0:T(512)(128)(4,1)S(1)}, pred[4]{0:T(512)(128)(4,1)}, u32[]{:S(2)}) copy-start(pred[4]{0:T(512)(128)(4,1)} %compare_and_fusion) | copy-start | bytes 16
  162.5 4.4 %copy-start.3 = (bf16[512,4,64]{0,2,1:T(8,128)(2,1)S(1)}, bf16[512,4,64]{0,2,1:T(8,128)(2,1)}, u32[]{:S(2)}) copy-start(bf16[512,4,64]{0,2,1:T(8,128)(2,1)} %copy-done.2) | copy-start | bytes 786436
  168.4 1.7 copy-start.4
  249.8 5.6 %copy-start.7 = (f32[128,2]{0,1:T(2,128)S(1)}, f32[128,2]{0,1:T(2,128)}, u32[]{:S(2)}) copy-start(f32[128,2]{0,1:T(2,128)} %param.24) | copy-start | bytes 3076
  249.8 5.8 %copy-start.6 = (s32[128,2]{1,0:T(8,128)S(1)}, s32[128,2]{1,0:T(8,128)}, u32[]{:S(2)}) copy-start(s32[128,2]{1,0:T(8,128)} %copy-done.5) | copy-start | bytes 3076
  249.8 42.5 %all-to-all-start.2 = ((bf16[8,48,2048]{2,1,0:T(8,128)(2,1)}), bf16[8,48,2048]{2,1,0:T(8,128)(2,1)}, u32[]{:S(2)}, u32[]{:S(2)}) async-start(bf16[8,48,2048]{2,1,0:T(8,128)(2,1)} %bitcast.147), calls=%async_computation.3 | async-start | bytes 3145728 | tf_op jit(solution)/shard_map/all_to_all | solution.py:164
Sparse Core Ops, SparseCore 0:
  66.7 45.3 all-gather.1
  175.7 43.6 reduce-scatter.1
where the time goes:
time: 309 us; the launch traced here: 308 us
  waiting for transfers between devices  123 us (40%)
  local copies, waits for them, and re-layouts  49.6 us (16%)
  blocking collectives  44.1 us (14%)
  matrix products  42.6 us (14%)
  other arithmetic  19.3 us (6%)
  starting transfers between devices  15.1 us (5%)
  between operations  14.4 us (5%)
    all_to_all x1, waiting for transfers between devices, on_device(): lax.all_to_all(partial_value, 'tp', split_axis=0, concat_axis=0, tiled=True)  68.5 us
    all_to_all x1, blocking collectives, on_device(): lax.all_to_all(slot_rows, 'ep', split_axis=0, concat_axis=0, tiled=True)  44.1 us
    all_to_all x1, waiting for transfers between devices, on_device(): lax.all_to_all(summed, 'ep', split_axis=0, concat_axis=0, tiled=True)  33.4 us
    all_gather x1, waiting for transfers between devices, on_device(): lax.all_gather(arrived, 'tp', axis=0, tiled=True)  20.8 us
    dot_general x1, matrix products, on_device(): jnp.einsum('aecf,efd->aecd', hidden_units, down_weight, preferred_element...  14.2 us
    reshape x1, local copies, waits for them, and re-layouts, on_device(): partial_value.reshape(tp_size, ep_size * local_experts * capacity, -1)  10.7 us
    dot_general x1, matrix products, expert_hidden(): jnp.einsum('aecd,edf->aecf', piece, up_weight, preferred_element_type=jnp...  10.2 us
    convert_element_type x1, local copies, waits for them, and re-layouts, on_device(): partial_value = jnp.einsum('aecf,efd->aecd', hidden_units, down_weight, p...  9.65 us
  transfers between devices with their start and end apart: 5, of which 3 were waited for; matrix products, arithmetic and copies ran while one was open for 31% of the time, Pallas kernels for 0%

commit v1 on v0

--- a/solution.py
+++ b/solution.py
@@ -1,6 +1,8 @@
 import jax
 import jax.numpy as jnp
 from jax import lax
+from jax.experimental import pallas as pl
+from jax.experimental.pallas import tpu as pltpu
 from jax.sharding import PartitionSpec as P
 
 EXPERTS = 32
@@ -106,6 +108,329 @@
     clipped = jnp.minimum(gate_pre, CLAMP_LIMIT)
     linear = jnp.clip(up_pre, -CLAMP_LIMIT, CLAMP_LIMIT)
     return (clipped * jax.nn.sigmoid(ACT_SLOPE * clipped) * (linear + 1.0)).astype(jnp.bfloat16)
+
+
+MESH = pl.DeviceIdType.MESH
+
+
+def activation(gate_pre, up_pre):
+    clipped = jnp.minimum(gate_pre, CLAMP_LIMIT)
+    linear = jnp.clip(up_pre, -CLAMP_LIMIT, CLAMP_LIMIT)
+    return (clipped * jax.nn.sigmoid(ACT_SLOPE * clipped) * (linear + 1.0)).astype(jnp.bfloat16)
+
+
+def expert_kernel(
+    dims, slots, perm, unperm, gate_hbm, up_hbm, down_hbm, ret,
+    gate_w, up_w, down_w, gath, xbuf, part, dbuf, sums, ybuf,
+    wsem, local_sem, zs, zr, ys, yr, ds, dr, rds, rdr, rys, ryr, rzs, rzr,
+):
+    ep, half, local, cap, rows, width, ffn = dims
+    group = 2 * half * cap
+    lot = ep // 2
+    me = lax.axis_index("ep")
+    tp = lax.axis_index("tp")
+    hi, core = tp // 2, tp % 2
+    other = 1 - core
+    partner = hi * 2 + other
+
+    weights = [
+        pltpu.make_async_copy(gate_hbm, gate_w, wsem.at[0]),
+        pltpu.make_async_copy(up_hbm, up_w, wsem.at[1]),
+        pltpu.make_async_copy(down_hbm, down_w, wsem.at[2]),
+    ]
+    own = pltpu.make_async_copy(slots.at[me], gath.at[me, hi, core], local_sem.at[0])
+    own.start()
+
+    barrier = pltpu.get_barrier_semaphore()
+    for step in range(1, ep):
+        pl.semaphore_signal(barrier, inc=1, device_id=((me + step) % ep, tp), device_id_type=MESH)
+    for j in range(1, half):
+        pl.semaphore_signal(
+            barrier, inc=1, device_id=(me, (hi + j) % half * 2 + core), device_id_type=MESH
+        )
+    pl.semaphore_signal(barrier, inc=1, device_id=(me, partner), device_id_type=MESH)
+    pl.semaphore_wait(barrier, ep - 1 + half - 1 + 1)
+
+    def source(d):
+        return (me - d + ep) % ep
+
+    def z_copy(d):
+        target = (me + d) % ep
+        return pltpu.make_async_remote_copy(
+            src_ref=slots.at[target], dst_ref=gath.at[me, hi, core],
+            send_sem=zs.at[d], recv_sem=zr.at[d], device_id=(target, tp), device_id_type=MESH,
+        )
+
+    def y_copy(d, j):
+        s = source(d)
+        return pltpu.make_async_remote_copy(
+            src_ref=gath.at[s, hi, core], dst_ref=gath.at[s, hi, core],
+            send_sem=ys.at[d, j], recv_sem=yr.at[d, j],
+            device_id=(me, (hi + j) % half * 2 + core), device_id_type=MESH,
+        )
+
+    def d_copy(d, j):
+        s = source(d)
+        block = (hi - j + half) % half
+        return pltpu.make_async_remote_copy(
+            src_ref=gath.at[s, block, core], dst_ref=gath.at[s, block, core],
+            send_sem=ds.at[d, j], recv_sem=dr.at[d, j],
+            device_id=(me, partner), device_id_type=MESH,
+        )
+
+    def rd_copy(d, h):
+        s = source(d)
+        return pltpu.make_async_remote_copy(
+            src_ref=part.at[s, h, other], dst_ref=dbuf.at[s, h],
+            send_sem=rds.at[d, h], recv_sem=rdr.at[d, h],
+            device_id=(me, partner), device_id_type=MESH,
+        )
+
+    def ry_copy(d, j):
+        s = source(d)
+        h = (hi + j) % half
+        return pltpu.make_async_remote_copy(
+            src_ref=sums.at[s, h], dst_ref=ybuf.at[s, j],
+            send_sem=rys.at[d, j], recv_sem=ryr.at[d, j],
+            device_id=(me, h * 2 + core), device_id_type=MESH,
+        )
+
+    def rz_copy(d):
+        s = source(d)
+        return pltpu.make_async_remote_copy(
+            src_ref=sums.at[s, hi], dst_ref=ret.at[me],
+            send_sem=rzs.at[d], recv_sem=rzr.at[d], device_id=(s, tp), device_id_type=MESH,
+        )
+
+    def each(first, last, body):
+        lax.fori_loop(first, last, lambda i, carry: (body(i), carry)[1], 0)
+
+    each(1, ep, lambda d: z_copy(d).start())
+    for copy in weights:
+        copy.start()
+
+    def pass_on(d):
+        for j in range(1, half):
+            y_copy(d, j).start()
+        d_copy(d, 0).start()
+
+    def hand_over(d):
+        for j in range(1, half):
+            y_copy(d, j).wait_recv()
+            d_copy(d, j).start()
+
+    def forward(d):
+        z_copy(d).wait_recv()
+        pass_on(d)
+        hand_over(d - 1)
+
+    own.wait()
+    pass_on(0)
+    each(1, lot, forward)
+
+    tile = min(width, 512)
+
+    def arrange(d, base):
+        for j in range(half):
+            d_copy(d, j).wait_recv()
+        s = source(d)
+        at = pl.multiple_of((d - base) * group, 16)
+        for col in range(0, width, tile):
+            block = gath[s, :, :, :, col : col + tile].reshape(2 * half * rows, tile)
+            sorted_rows = jnp.dot(perm[...], block, preferred_element_type=jnp.float32)
+            sorted_rows = sorted_rows.astype(jnp.bfloat16)
+            for e in range(local):
+                xbuf[e, pl.ds(at, group), col : col + tile] = sorted_rows[
+                    e * group : (e + 1) * group
+                ]
+
+    def expert(e):
+        x = xbuf[e]
+        hidden = activation(
+            jnp.dot(x, gate_w[e], preferred_element_type=jnp.float32),
+            jnp.dot(x, up_w[e], preferred_element_type=jnp.float32),
+        )
+        for col in range(0, width, tile):
+            xbuf[e, :, col : col + tile] = jnp.dot(
+                hidden, down_w[e, :, col : col + tile], preferred_element_type=jnp.float32
+            ).astype(jnp.bfloat16)
+
+    def split(d, base):
+        s = source(d)
+        at = pl.multiple_of((d - base) * group, 16)
+        for col in range(0, width, tile):
+            block = jnp.concatenate(
+                [xbuf[e, pl.ds(at, group), col : col + tile] for e in range(local)], axis=0
+            )
+            back = jnp.dot(unperm[...], block, preferred_element_type=jnp.float32)
+            part[s, :, :, :, col : col + tile] = back.astype(jnp.bfloat16).reshape(
+                half, 2, rows, tile
+            )
+        for h in range(half):
+            rd_copy(d, h).start()
+
+    def join(d):
+        s = source(d)
+        for h in range(half):
+            rd_copy(d, h).wait_recv()
+            sums[s, h] = (
+                part[s, h, core].astype(jnp.float32) + dbuf[s, h].astype(jnp.float32)
+            ).astype(jnp.bfloat16)
+        for j in range(1, half):
+            ry_copy(d, j).start()
+
+    def finish(d):
+        s = source(d)
+        total = part[s, hi, core].astype(jnp.float32) + dbuf[s, hi].astype(jnp.float32)
+        for j in range(1, half):
+            ry_copy(d, j).wait_recv()
+            total = total + ybuf[s, j].astype(jnp.float32)
+        sums[s, hi] = total.astype(jnp.bfloat16)
+
+    def give_back(d):
+        finish(d)
+        rz_copy(d).start()
+
+    hand_over(lot - 1)
+    each(0, lot, lambda d: arrange(d, 0))
+    for copy in weights:
+        copy.wait()
+
+    share = lot // local
+
+    def forward_late(d):
+        z_copy(d).wait_recv()
+        pass_on(d)
+
+        @pl.when(d > lot)
+        def _():
+            hand_over(d - 1)
+
+    def first_expert(e):
+        expert(e)
+        for i in range(share):
+            forward_late(lot + e * share + i)
+
+    each(0, local, first_expert)
+    each(lot + local * share, ep, forward_late)
+
+    def split_join(d, base, first):
+        split(d, base)
+
+        @pl.when(d > first)
+        def _():
+            join(d - 1)
+
+    each(0, lot, lambda d: split_join(d, 0, 0))
+    join(lot - 1)
+    hand_over(ep - 1)
+    each(lot, ep, lambda d: arrange(d, lot))
+
+    finish(0)
+    mine = pltpu.make_async_copy(sums.at[me, hi], ret.at[me], local_sem.at[1])
+    mine.start()
+
+    def give_early(d):
+        @pl.when(d > 0)
+        def _():
+            give_back(d)
+
+    def second_expert(e):
+        expert(e)
+        for i in range(share):
+            give_early(e * share + i)
+
+    each(0, local, second_expert)
+    each(local * share, lot, give_early)
+    each(lot, ep, lambda d: split_join(d, lot, lot))
+    join(ep - 1)
+    each(lot, ep, give_back)
+    mine.wait()
+
+    def drain(d):
+        for j in range(1, half):
+            y_copy(d, j).wait_send()
+            ry_copy(d, j).wait_send()
+        for j in range(half):
+            d_copy(d, j).wait_send()
+            rd_copy(d, j).wait_send()
+
+    def drain_far(d):
+        z_copy(d).wait_send()
+        rz_copy(d).wait()
+
+    each(0, ep, drain)
+    each(1, ep, drain_far)
+
+
+def run_experts(slots, dims, gate_weight, up_weight, down_weight):
+    ep, half, local, cap, rows, width, ffn = dims
+    tps = 2 * half
+    wide = tps * rows
+    order = jnp.arange(local * tps * cap)
+    e, t, c = order // (tps * cap), order // cap % tps, order % cap
+    perm = (t * rows + e * cap + c)[:, None] == jnp.arange(wide)[None, :]
+    perm = perm.astype(jnp.bfloat16)
+    dma = pltpu.SemaphoreType.DMA
+    bf = jnp.bfloat16
+    vm = pl.BlockSpec(memory_space=pltpu.VMEM)
+    anys = pl.BlockSpec(memory_space=pl.ANY)
+    copies = ep * tps * local * cap
+    return pl.pallas_call(
+        lambda *refs: expert_kernel(dims, *refs),
+        name="expert_exchange",
+        out_shape=jax.ShapeDtypeStruct((ep, rows, width), bf),
+        in_specs=[vm, vm, vm, anys, anys, anys],
+        out_specs=vm,
+        scratch_shapes=[
+            pltpu.VMEM((local, width, ffn), bf),
+            pltpu.VMEM((local, width, ffn), bf),
+            pltpu.VMEM((local, ffn, width), bf),
+            pltpu.VMEM((ep, half, 2, rows, width), bf),
+            pltpu.VMEM((local, ep // 2 * tps * cap, width), bf),
+            pltpu.VMEM((ep, half, 2, rows, width), bf),
+            pltpu.VMEM((ep, half, rows, width), bf),
+            pltpu.VMEM((ep, half, rows, width), bf),
+            pltpu.VMEM((ep, half, rows, width), bf),
+            dma((3,)),
+            dma((2,)),
+            dma((ep,)), dma((ep,)),
+            dma((ep, half)), dma((ep, half)),
+            dma((ep, half)), dma((ep, half)),
+            dma((ep, half)), dma((ep, half)),
+            dma((ep, half)), dma((ep, half)),
+            dma((ep,)), dma((ep,)),
+        ],
+        compiler_params=pltpu.CompilerParams(
+            collective_id=0, has_side_effects=True, vmem_limit_bytes=67043328
+        ),
+        cost_estimate=pl.CostEstimate(
+            flops=6 * copies * width * ffn, bytes_accessed=120000000, transcendentals=0
+        ),
+    )(slots, perm, perm.T, gate_weight, up_weight, down_weight)
+
+
+def fits(dims):
+    ep, half, local, cap, rows, width, ffn = dims
+    if half < 1 or ep % 2 or rows % 16 or (2 * half * cap) % 16:
+        return False
+    held = 3 * local * width * ffn + ep * half * rows * width * 7
+    held += ep * half * local * cap * width + 2 * ep * rows * width
+    return 2 * held < 60 * 1024 * 1024
+
+
+def slot_of(routes, cap):
+    flat = routes.reshape(-1)
+    hot = flat[:, None] == lax.broadcasted_iota(jnp.int32, (1, EXPERTS), 1)
+    count = flat.shape[0]
+    earlier = lax.broadcasted_iota(jnp.int32, (count, count), 0) > lax.broadcasted_iota(
+        jnp.int32, (count, count), 1
+    )
+    before = jnp.dot(
+        earlier.astype(jnp.bfloat16), hot.astype(jnp.bfloat16), preferred_element_type=jnp.float32
+    )
+    position = jnp.sum(jnp.where(hot, before, 0.0), axis=1).astype(jnp.int32)
+    return (flat * cap + position).reshape(routes.shape)
 
 
 def on_device(
@@ -125,11 +450,8 @@
     down_weight,
 ):
     heads_out = attend(query_rows, key_rows, value_rows, query_gain, key_gain, sink_logits)
-    attended = lax.psum_scatter(
-        jnp.dot(heads_out, out_weight, preferred_element_type=jnp.float32).astype(jnp.bfloat16),
-        "tp",
-        scatter_dimension=0,
-        tiled=True,
+    projected = jnp.dot(heads_out, out_weight, preferred_element_type=jnp.float32).astype(
+        jnp.bfloat16
     )
     own_rows = expert_input.shape[0]
     fanout = routes.shape[1]
@@ -144,29 +466,57 @@
         * expert_gain
     ).astype(jnp.bfloat16)
     route_weight = jax.nn.softmax(route_logits, axis=-1)
-    combine = combine_matrix(routes, route_weight, capacity)
-    sender = dispatch_matrix(routes, capacity)
-    slot_rows = jnp.einsum(
-        "ecr,rd->ecd", sender, normed, preferred_element_type=jnp.float32
-    ).astype(jnp.bfloat16)
-    slot_rows = slot_rows.reshape(ep_size, local_experts, capacity, -1)
-    arrived = lax.all_to_all(slot_rows, "ep", split_axis=0, concat_axis=0, tiled=True)
-    hidden_units = expert_hidden(
-        lax.all_gather(arrived, "tp", axis=0, tiled=True), gate_weight, up_weight
-    )
-    partial_value = jnp.einsum(
-        "aecf,efd->aecd", hidden_units, down_weight, preferred_element_type=jnp.float32
-    ).astype(jnp.bfloat16)
-    partial_value = partial_value.reshape(tp_size, ep_size * local_experts * capacity, -1)
-    pieces = lax.all_to_all(partial_value, "tp", split_axis=0, concat_axis=0, tiled=True)
-    summed = jnp.sum(pieces, axis=0, dtype=jnp.float32).astype(jnp.bfloat16)
-    summed = summed.reshape(ep_size, local_experts * capacity, -1)
-    returned = lax.all_to_all(summed, "ep", split_axis=0, concat_axis=0, tiled=True).reshape(
-        EXPERTS, capacity, -1
-    )
-    expert_mix = jnp.einsum(
-        "rec,ecd->rd", combine, returned.astype(jnp.float32), precision=lax.Precision.HIGHEST
-    ).astype(jnp.bfloat16)
+    dims = (
+        ep_size, tp_size // 2, local_experts, capacity, local_experts * capacity,
+        expert_input.shape[1], gate_weight.shape[2],
+    )
+    if fits(dims):
+        slot = slot_of(routes, capacity)
+        places = lax.broadcasted_iota(jnp.int32, (1, EXPERTS * capacity), 1)
+        sender = jnp.zeros((own_rows, EXPERTS * capacity), jnp.bool_)
+        combine = jnp.zeros((own_rows, EXPERTS * capacity), jnp.float32)
+        for k in range(fanout):
+            taken = slot[:, k : k + 1] == places
+            sender = sender | taken
+            combine = combine + jnp.where(taken, route_weight[:, k : k + 1], 0.0)
+        slot_rows = lax.dot_general(
+            sender.astype(jnp.bfloat16), normed, (((0,), (0,)), ((), ())),
+            preferred_element_type=jnp.float32,
+        ).astype(jnp.bfloat16)
+        slot_rows, projected = lax.optimization_barrier((slot_rows, projected))
+        attended = lax.psum_scatter(projected, "tp", scatter_dimension=0, tiled=True)
+        returned = run_experts(
+            slot_rows.reshape(ep_size, local_experts * capacity, -1), dims,
+            gate_weight, up_weight, down_weight,
+        ).reshape(EXPERTS * capacity, -1)
+        expert_mix = jnp.dot(
+            combine, returned.astype(jnp.float32), precision=lax.Precision.HIGHEST
+        ).astype(jnp.bfloat16)
+    else:
+        attended = lax.psum_scatter(projected, "tp", scatter_dimension=0, tiled=True)
+        combine = combine_matrix(routes, route_weight, capacity)
+        sender = dispatch_matrix(routes, capacity)
+        slot_rows = jnp.einsum(
+            "ecr,rd->ecd", sender, normed, preferred_element_type=jnp.float32
+        ).astype(jnp.bfloat16)
+        slot_rows = slot_rows.reshape(ep_size, local_experts, capacity, -1)
+        arrived = lax.all_to_all(slot_rows, "ep", split_axis=0, concat_axis=0, tiled=True)
+        hidden_units = expert_hidden(
+            lax.all_gather(arrived, "tp", axis=0, tiled=True), gate_weight, up_weight
+        )
+        partial_value = jnp.einsum(
+            "aecf,efd->aecd", hidden_units, down_weight, preferred_element_type=jnp.float32
+        ).astype(jnp.bfloat16)
+        partial_value = partial_value.reshape(tp_size, ep_size * local_experts * capacity, -1)
+        pieces = lax.all_to_all(partial_value, "tp", split_axis=0, concat_axis=0, tiled=True)
+        summed = jnp.sum(pieces, axis=0, dtype=jnp.float32).astype(jnp.bfloat16)
+        summed = summed.reshape(ep_size, local_experts * capacity, -1)
+        returned = lax.all_to_all(summed, "ep", split_axis=0, concat_axis=0, tiled=True).reshape(
+            EXPERTS, capacity, -1
+        )
+        expert_mix = jnp.einsum(
+            "rec,ecd->rd", combine, returned.astype(jnp.float32), precision=lax.Precision.HIGHEST
+        ).astype(jnp.bfloat16)
     return (attended, expert_mix)
 
 

time: 309 us -> 163 us (0.53)
  waiting for transfers between devices: 123 us -> 0.02 us
  Pallas kernels: 0 us -> 114 us
  blocking collectives: 44.1 us -> 0 us
  local copies, waits for them, and re-layouts: 49.6 us -> 8.25 us
  matrix products: 42.6 us -> 11.3 us
  other arithmetic: 19.3 us -> 8.93 us
  starting transfers between devices: 15.1 us -> 5.55 us
    pallas_call x0 -> x1, Pallas kernels: none -> 114 us  [run_experts(): pl.pallas_call(lambda *refs: expert_kernel(dims, *refs), name='expert_exc...]
    all_to_all x2 -> x0, waiting for transfers between devices: 102 us -> none  [the longest x1 68.5 us: on_device(): lax.all_to_all(partial_value, 'tp', split_axis=0, concat_axis=0, tiled=True)]
    all_to_all x1 -> x0, blocking collectives: 44.1 us -> none  [on_device(): lax.all_to_all(slot_rows, 'ep', split_axis=0, concat_axis=0, tiled=True)]
    dot_general x6 -> x3, matrix products: 36.7 us -> 5.31 us  [the longest x1 3.26 us: on_device(): jnp.dot(combine, returned.astype(jnp.float32), precision=lax.Precision.HI...]
    all_gather x1 -> x0, waiting for transfers between devices: 20.8 us -> none  [on_device(): lax.all_gather(arrived, 'tp', axis=0, tiled=True)]
    reshape x4 -> x0, local copies, waits for them, and re-layouts: 20.1 us -> none  [the longest x1 10.7 us: on_device(): partial_value.reshape(tp_size, ep_size * local_experts * capacity, -1)]
    all_to_all x2 -> x0, starting transfers between devices: 10.9 us -> none  [the longest x1 5.64 us: on_device(): lax.all_to_all(summed, 'ep', split_axis=0, concat_axis=0, tiled=True)]
    convert_element_type x1 -> x2, local copies, waits for them, and re-layouts: 9.65 us -> 0.19 us  [slot_of(): position = jnp.sum(jnp.where(hot, before, 0.0), axis=1).astype(jnp.int32)]
  transfers between devices with their start and end apart: 5 -> 2, of which waited for: 3 -> 0; matrix products, arithmetic and copies ran while one was open for 31% -> 9% of each run, Pallas kernels for 0% -> 70%
where the time goes in v1:
time: 163 us
  Pallas kernels  114 us (70%)
  between operations  14.5 us (9%)
  matrix products  11.3 us (7%)
  other arithmetic  8.93 us (5%)
  local copies, waits for them, and re-layouts  8.25 us (5%)
  starting transfers between devices  5.55 us (3%)
    pallas_call x1, Pallas kernels, run_experts(): pl.pallas_call(lambda *refs: expert_kernel(dims, *refs), name='expert_exc...  114 us
    ppermute x1, starting transfers between devices, shifted(): lax.ppermute(value, axis, [(source, source + steps) for source in range(i...  5.52 us
    unnamed x34, local copies, waits for them, and re-layouts  3.4 us
    dot_general x1, matrix products, on_device(): jnp.dot(combine, returned.astype(jnp.float32), precision=lax.Precision.HI...  3.26 us
  transfers between devices with their start and end apart: 2, of which 0 were waited for; matrix products, arithmetic and copies ran while one was open for 9% of the time, Pallas kernels for 70%

profile of v1, /device:TPU:0, one launch (start us, length us, event | category | flops | bytes accessed | tf_op | source)
XLA Modules:
  0.0 162.8 jit_solution(3600350288417380128)
XLA Ops:
  7.2 0.0 reduce-scatter.2.cloned.1.call-start
  7.2 1.2 copy.50
  8.4 0.1 multiply_reduce_fusion
  8.5 0.8 multiply_convert_fusion.1
  9.3 0.0 copy-start.2
  9.3 0.7 copy-done.2
  10.0 1.1 copy.51
  11.1 0.0 copy-start.4
  11.1 0.7 pad_maximum_fusion.2
  11.8 5.5 %collective-permute-start = (bf16[2,128,4,64]{1,3,2,0:T(8,128)(2,1)}, bf16[2,128,4,64]{1,3,2,0:T(8,128)(2,1)}, u32[]{:S(2)}, u32[]{:S(2)}) collective-permute-start(bf16[2,128,4,64]{1,3,2,0:T(8,128)(2,1)} %pad_maximum_fusion.2), channel_id=1, source_target_pairs={{0,4},{4,8},{8,12},{12,16},{16,20},{20,24},{24,28},{1,5},{5,9},{9,... | collective-permute-start | bytes 393224 | tf_op jit(solution)/shard_map/ppermute | solution.py:21
  17.3 0.2 reshape.176
  17.5 0.3 copy.54
  17.8 0.0 copy-start.10
  17.8 0.0 copy-start.14
  17.8 1.4 convert_multiply_fusion.2
  19.2 0.5 reshape.177
  19.7 1.2 reshape.184
  21.0 0.0 copy-start.8
  21.0 1.6 reduce_sum.57
  22.7 0.1 max.22
  22.8 0.3 copy.59
  23.1 0.1 copy.48
  23.2 0.1 eq.79
  23.4 0.2 fusion.12
  23.6 0.1 convert_element_type.55
  23.7 0.1 copy.49
  23.9 0.2 fusion.13
  24.1 0.1 fusion.26
  24.2 1.2 multiply_convert_fusion
  25.4 1.8 %convolution_convert_fusion.1 = bf16[384,2048]{1,0:T(8,128)(2,1)} fusion(bf16[128,2048]{1,0:T(8,128)(2,1)S(1)} %copy-done.1, f32[2048]{0:T(1024)S(1)} %copy-done.8, f32[128]{0:T(128)S(1)} %add_rsqrt_fusion.2, s32[128]{0:T(128)S(1)} %get-tuple-element.15, s32[128]{0:T(128)S(1)} %get-tuple-element.14), kind=kOutput, calls=%fused_computation.11 | convolution fusion | flops 203309056 | bytes 2106880 | tf_op jit(solution)/shard_map/dot_general | solution.py:482
  27.2 0.2 not_and_fusion
  27.4 0.9 slice_bitcast_fusion.1
  28.3 0.1 fusion.29
  28.4 0.1 copy.85
  28.5 1.1 fusion.2
  29.6 0.1 broadcast_maximum_fusion
  29.7 1.6 fusion
  31.3 0.1 add_bitcast_fusion
  31.4 0.1 copy.86
  31.4 0.0 copy-start
  31.5 1.6 fusion.9
  33.1 0.6 copy.61
  33.7 3.2 %convolution_convert_fusion = bf16[512,2048]{1,0:T(8,128)(2,1)} fusion(bf16[768,2048]{1,0:T(8,128)(2,1)S(1)} %copy-done, bf16[96,8,4,128]{3,2,1,0:T(4,128)(2,1)S(1)} %bitcast.79), kind=kOutput, calls=%fused_computation.10 | convolution fusion | flops 1611661312 | bytes 6029312 | tf_op jit(solution)/shard_map/dot_general | solution.py:453
  37.0 0.0 reduce-scatter.2.cloned.1.call-update
  37.1 0.6 slice_bitcast_fusion.4
  37.7 0.7 fusion.37
  38.4 114.3 %expert_exchange.1 = bf16[8,48,2048]{2,1,0:T(8,128)(2,1)} custom-call(bf16[8,48,2048]{2,1,0:T(8,128)(2,1)} %bitcast.81, bf16[192,192]{1,0:T(8,128)(2,1)} %get-tuple-element.13.refs_1_, bf16[192,192]{1,0:T(8,128)(2,1)} %get-tuple-element.12.refs_2_, bf16[4,2048,512]{2,1,0:T(8,128)(2,1)} %refs_3_.1, bf16[4,2048,512]{2,1,0:T(8,128)(2,1)} %refs_4_.1, ...), custom_call_target="tpu_custom_call" | custom-call | flops 9663676416 | bytes 120000000 | tf_op jit(solution)/shard_map/expert_exchange/pallas_call | solution.py:379
  152.7 3.3 %convolution_convert_fusion.2 = bf16[128,2048]{1,0:T(8,128)(2,1)} fusion(bf16[384,2048]{1,0:T(8,128)(2,1)} %bitcast.80, f32[128]{0:T(128)} %get-tuple-element.11, f32[128]{0:T(128)} %get-tuple-element.10, s32[128]{0:T(128)} %copy-done.12, s32[128]{0:T(128)} %copy-done.11), kind=kOutput, calls=%fused_computation.12 | convolution fusion | flops 1208467456 | bytes 2099200 | tf_op jit(solution)/shard_map/dot_general | solution.py:492
  (43 shorter events, 0.3 us)
Async XLA Ops:
  7.2 10.3 %copy-start.6 = (bf16[512,768]{1,0:T(8,128)(2,1)S(1)}, bf16[512,768]{1,0:T(8,128)(2,1)}, u32[]{:S(2)}) copy-start(bf16[512,768]{1,0:T(8,128)(2,1)} %param.14) | copy-start | bytes 2359300
  7.2 148.8 %reduce-scatter.2.cloned.1.call-start = ((), (), s32[]{:S(2)}) async-start(), calls=%async_computation.1 | async-start | bytes 2621440 | tf_op jit(solution)/shard_map/reduce_scatter | solution.py:487
  9.3 0.7 copy-start.2
  11.1 6.7 %copy-start.4 = (bf16[512,256]{0,1:T(8,128)(2,1)}, bf16[512,256]{0,1:T(8,128)(2,1)S(1)}, u32[]{:S(2)}) copy-start(bf16[512,256]{0,1:T(8,128)(2,1)S(1)} %copy.51) | copy-start | bytes 786436
  11.8 15.6 %collective-permute-start = (bf16[2,128,4,64]{1,3,2,0:T(8,128)(2,1)}, bf16[2,128,4,64]{1,3,2,0:T(8,128)(2,1)}, u32[]{:S(2)}, u32[]{:S(2)}) collective-permute-start(bf16[2,128,4,64]{1,3,2,0:T(8,128)(2,1)} %pad_maximum_fusion.2), channel_id=1, source_target_pairs={{0,4},{4,8},{8,12},{12,16},{16,20},{20,24},{24,28},{1,5},{5,9},{9,... | collective-permute-start | bytes 393224 | tf_op jit(solution)/shard_map/ppermute | solution.py:21
  17.8 4.8 %copy-start.10 = (f32[12,64]{1,0:T(8,128)S(1)}, f32[12,64]{1,0:T(8,128)}, u32[]{:S(2)}) copy-start(f32[12,64]{1,0:T(8,128)} %param.17) | copy-start | bytes 9220
  17.8 4.9 %copy-start.14 = (f32[12]{0:T(128)S(1)}, f32[12]{0:T(128)}, u32[]{:S(2)}) copy-start(f32[12]{0:T(128)} %param.19) | copy-start | bytes 148
  19.2 3.9 %copy-start.13 = (s32[128,2]{0,1:T(2,128)S(1)}, s32[128,2]{0,1:T(2,128)}, u32[]{:S(2)}) copy-start(s32[128,2]{0,1:T(2,128)} %param.23) | copy-start | bytes 3076
  19.2 4.6 %copy-start.1 = (bf16[128,2048]{1,0:T(8,128)(2,1)S(1)}, bf16[128,2048]{1,0:T(8,128)(2,1)}, u32[]{:S(2)}) copy-start(bf16[128,2048]{1,0:T(8,128)(2,1)} %param.21) | copy-start | bytes 1572868
  19.2 4.8 %copy-start.9 = (f32[4,64]{1,0:T(4,128)S(1)}, f32[4,64]{1,0:T(4,128)}, u32[]{:S(2)}) copy-start(f32[4,64]{1,0:T(4,128)} %param.18) | copy-start | bytes 3076
  21.0 4.4 %copy-start.8 = (f32[2048]{0:T(1024)S(1)}, f32[2048]{0:T(1024)}, u32[]{:S(2)}) copy-start(f32[2048]{0:T(1024)} %param.22) | copy-start | bytes 24580
  23.8 4.5 %copy-start.3 = (bf16[512,4,64]{0,2,1:T(8,128)(2,1)S(1)}, bf16[512,4,64]{0,2,1:T(8,128)(2,1)}, u32[]{:S(2)}) copy-start(bf16[512,4,64]{0,2,1:T(8,128)(2,1)} %copy-done.2) | copy-start | bytes 786436
  23.8 4.5 %copy-start.5 = (bf16[512,256]{0,1:T(8,128)(2,1)S(1)}, bf16[512,256]{0,1:T(8,128)(2,1)}, u32[]{:S(2)}) copy-start(bf16[512,256]{0,1:T(8,128)(2,1)} %copy-done.4) | copy-start | bytes 786436
  23.8 3.5 %copy-start.11 = (s32[128]{0:T(128)}, s32[128]{0:T(128)S(1)}, u32[]{:S(2)}) copy-start(s32[128]{0:T(128)S(1)} %get-tuple-element.14) | copy-start | bytes 1540
  23.9 3.5 %copy-start.12 = (s32[128]{0:T(128)}, s32[128]{0:T(128)S(1)}, u32[]{:S(2)}) copy-start(s32[128]{0:T(128)S(1)} %get-tuple-element.15) | copy-start | bytes 1540
  31.4 2.3 %copy-start = (bf16[768,2048]{1,0:T(8,128)(2,1)S(1)}, bf16[768,2048]{1,0:T(8,128)(2,1)}, u32[]{:S(2)}) copy-start(bf16[768,2048]{1,0:T(8,128)(2,1)} %param.20) | copy-start | bytes 9437188
  33.7 3.3 %copy-start.7 = (f32[128,2]{0,1:T(2,128)S(1)}, f32[128,2]{0,1:T(2,128)}, u32[]{:S(2)}) copy-start(f32[128,2]{0,1:T(2,128)} %param.24) | copy-start | bytes 3076
Sparse Core Ops, SparseCore 0:
  37.1 35.9 reduce-scatter.1
